TPU v7x, 32 devices: a whole 2x2x4 slice. The times are simulated.
32 devices in a mesh: grp: 2 (over y), sp: 4 (over z), tp: 4 (over x, core).
Axes of the slice: x: 2, y: 2, z: 4, core: 2. Of those that a mesh axis runs over, the one named last changes fastest.
Arguments:
- hidden_in: bfloat16 [2048, 2048], P(('grp', 'sp')), parts along dimension 0, may hold values from -6 to 6
- query_latent_rows: bfloat16 [2048, 768], P(('grp', 'sp')), parts along dimension 0, may hold values from -6 to 6
- key_value_latent: bfloat16 [2048, 512], P(('grp', 'sp')), parts along dimension 0, may hold values from -6 to 6
- rotary_key: bfloat16 [2048, 32], P(('grp', 'sp')), parts along dimension 0, may hold values from -64 to 64
- query_norm_gain: float32 [768], replicated, may hold values from 0.1 to 1.9
- key_value_gain: float32 [512], replicated, may hold values from 0.1 to 1.9
- query_up_weight: bfloat16 [768, 1536], P(None, 'tp'), may hold values from -0.625 to 0.625
- key_value_up_weight: bfloat16 [512, 2048], P(None, 'tp'), may hold values from -0.25 to 0.25
- out_proj: bfloat16 [1024, 2048], P('tp'), may hold values from -0.1875 to 0.1875
- feed_gain: float32 [2048], replicated, may hold values from 0.1 to 1.9
- feed_up: bfloat16 [2048, 8192], P('sp', 'tp'), may hold values from -0.125 to 0.125
- feed_down: bfloat16 [8192, 2048], P('tp', 'sp'), may hold values from -0.0625 to 0.0625
Outputs:
- layer_out: bfloat16 [2048, 2048], P(('grp', 'sp', 'tp')), parts along dimension 0
There are 2 independent parts, one for each index of `grp`. A program takes and returns all parts, laid end to end along the dimension named above; an argument that names none is the same for every part. Nothing has to cross between parts.
All inputs are finite; a program needn't handle non-finite values.
Results may differ from a plain program's by a relative error of at most 0.02.
Values may be sent and summed in bfloat16 or wider, within the bound.
A program may use at most 128 MiB of HBM per device.

v0:
```python
import math
import jax
import jax.numpy as jnp
from jax import lax
from jax.sharding import PartitionSpec as P

QUERY_KEY_PLAIN = 64
QUERY_KEY_ROTARY = 32
VALUE_HEAD_SIZE = 64


def normalize(values, gain):
    floats = values.astype(jnp.float32)
    return floats * lax.rsqrt(jnp.mean(floats * floats, axis=-1, keepdims=True) + 1e-06) * gain


def rotate(values, position):
    half_size = values.shape[-1] // 2
    inverse = 10000.0 ** (-jnp.arange(half_size, dtype=jnp.float32) * 2.0 / values.shape[-1])
    angles = position[:, None] * inverse[None, :]
    cosine = jnp.concatenate([jnp.cos(angles), jnp.cos(angles)], axis=-1)
    sine = jnp.concatenate([jnp.sin(angles), jnp.sin(angles)], axis=-1)
    shape = (values.shape[0],) + (1,) * (values.ndim - 2) + (values.shape[-1],)
    turned = jnp.concatenate([-values[..., half_size:], values[..., :half_size]], axis=-1)
    return values * cosine.reshape(shape) + turned * sine.reshape(shape)


def on_device(
    hidden_in,
    query_latent_rows,
    key_value_latent,
    rotary_key,
    query_norm_gain,
    key_value_gain,
    query_up_weight,
    key_value_up_weight,
    out_proj,
    feed_gain,
    feed_up,
    feed_down,
):
    tokens_here = hidden_in.shape[0]
    heads_here = query_up_weight.shape[1] // (QUERY_KEY_PLAIN + QUERY_KEY_ROTARY)
    position = (lax.axis_index("sp") * tokens_here + jnp.arange(tokens_here)).astype(jnp.float32)
    scale_factor = (QUERY_KEY_PLAIN + QUERY_KEY_ROTARY) ** (-0.5)
    query_norm = normalize(query_latent_rows, query_norm_gain).astype(jnp.bfloat16)
    queries = jnp.dot(query_norm, query_up_weight, preferred_element_type=jnp.float32).reshape(
        tokens_here, heads_here, QUERY_KEY_PLAIN + QUERY_KEY_ROTARY
    )
    queries = jnp.concatenate(
        [queries[..., :QUERY_KEY_PLAIN], rotate(queries[..., QUERY_KEY_PLAIN:], position)], axis=-1
    ).astype(jnp.bfloat16)
    query_plain = queries[..., :QUERY_KEY_PLAIN]
    query_turned = queries[..., QUERY_KEY_PLAIN:]
    latent = normalize(key_value_latent, key_value_gain).astype(jnp.bfloat16)
    key_rope = rotate(rotary_key.astype(jnp.float32), position).astype(jnp.bfloat16)

    def attend_block(carry, key_plain, value_rows, rope_rows):
        row_max, denom, accum = carry
        scores = jnp.einsum(
            "qhd,khd->hqk", query_plain, key_plain, preferred_element_type=jnp.float32
        )
        scores = scores + jnp.einsum(
            "qhd,kd->hqk", query_turned, rope_rows, preferred_element_type=jnp.float32
        )
        scores = scores * scale_factor
        new_max = jnp.maximum(row_max, jnp.max(scores, axis=-1))
        expo = jnp.exp(scores - new_max[:, :, None])
        factor = jnp.exp(row_max - new_max)
        denom = denom * factor + jnp.sum(expo, axis=-1)
        update = jnp.einsum(
            "hqk,khd->qhd",
            expo.astype(jnp.bfloat16),
            value_rows,
            preferred_element_type=jnp.float32,
        )
        accum = accum * jnp.transpose(factor)[:, :, None] + update
        return (new_max, denom, accum)

    start_carry = (
        jnp.full((heads_here, tokens_here), -1e30, jnp.float32),
        jnp.zeros((heads_here, tokens_here), jnp.float32),
        jnp.zeros((tokens_here, heads_here, VALUE_HEAD_SIZE), jnp.float32),
    )
    own_keys = jnp.dot(latent, key_value_up_weight, preferred_element_type=jnp.float32).astype(
        jnp.bfloat16
    )
    pieces = (
        lax.all_gather(own_keys, "sp", axis=0, tiled=True),
        lax.all_gather(key_rope, "sp", axis=0, tiled=True),
    )
    rows_in = pieces[0].shape[0]
    block = math.gcd(rows_in, 1024)

    def step_block(index, inner):
        first = index * block
        bulk = lax.dynamic_slice_in_dim(pieces[0], first, block, 0)
        rope_rows = lax.dynamic_slice_in_dim(pieces[1], first, block, 0)
        bulk = bulk.reshape(block, heads_here, QUERY_KEY_PLAIN + VALUE_HEAD_SIZE)
        return attend_block(
            inner, bulk[..., :QUERY_KEY_PLAIN], bulk[..., QUERY_KEY_PLAIN:], rope_rows
        )

    final_carry = lax.fori_loop(0, rows_in // block, step_block, start_carry)
    denom = final_carry[1]
    accum = final_carry[2]
    mixed = (
        (accum / jnp.transpose(denom)[:, :, None])
        .astype(jnp.bfloat16)
        .reshape(tokens_here, heads_here * VALUE_HEAD_SIZE)
    )
    share = tokens_here // lax.axis_size("tp")
    lead = lax.axis_index("tp") * share
    branch = lax.psum(
        jnp.dot(mixed, out_proj, preferred_element_type=jnp.float32).astype(jnp.bfloat16), "tp"
    ).astype(jnp.float32)
    middle = (hidden_in.astype(jnp.float32) + branch).astype(jnp.bfloat16)
    normed = normalize(middle, feed_gain).astype(jnp.bfloat16)
    middle_own = lax.dynamic_slice_in_dim(middle, lead, share, 0)
    upward = jnp.dot(
        normed,
        lax.all_gather(feed_up, "sp", axis=0, tiled=True),
        preferred_element_type=jnp.float32,
    )
    activated = jnp.square(jax.nn.relu(upward)).astype(jnp.bfloat16)
    partial_sum = jnp.dot(
        activated,
        lax.all_gather(feed_down, "sp", axis=1, tiled=True),
        preferred_element_type=jnp.float32,
    )
    feed = lax.psum_scatter(
        partial_sum.astype(jnp.bfloat16), "tp", scatter_dimension=0, tiled=True
    ).astype(jnp.float32)
    return (middle_own.astype(jnp.float32) + feed).astype(jnp.bfloat16)


def solution(mesh):
    return jax.shard_map(
        on_device,
        mesh=mesh,
        in_specs=(
            P(("grp", "sp"), None),
            P(("grp", "sp"), None),
            P(("grp", "sp"), None),
            P(("grp", "sp"), None),
            P(),
            P(),
            P(None, "tp"),
            P(None, "tp"),
            P("tp", None),
            P(),
            P("sp", "tp"),
            P("tp", "sp"),
        ),
        out_specs=P(("grp", "sp", "tp"), None),
        check_vma=False,
    )
```

profile of v0, /device:TPU:0, one launch (start us, length us, event | category | flops | bytes accessed | tf_op | source)
XLA Modules:
  0.0 427.3 jit_solution(10657204658215220777)
XLA Ops:
  6.5 0.0 copy-start
  6.5 0.0 all-gather.4.cloned.1.call-start
  6.5 1.2 fusion.31
  7.7 2.2 convolution_convert_fusion.2
  9.9 0.0 all-gather.4.cloned.1.call-update
  9.9 0.0 all-reduce.2.cloned.1.call-start
  10.0 0.7 convert_element_type.75
  10.7 0.7 slice.45
  11.4 0.1 multiply_cosine_fusion
  11.6 0.7 pad_maximum_fusion
  12.3 15.3 %all_gather.13 = bf16[1024,32]{0,1:T(8,128)(2,1)S(1)} all-gather(bf16[256,32]{0,1:T(8,128)(2,1)S(1)} %get-tuple-element.26), channel_id=1, replica_groups=mesh['grp'=2,'sp'=4,'tp'=4] {'sp'}, dimensions={0}, use_global_device_ids=true | all-gather | bytes 81920 | tf_op jit(solution)/shard_map/all_gather | solution.py:90
  27.6 1.2 fusion.26
  28.8 1.6 fusion.37
  30.4 11.1 %all-gather.4.cloned.1.call-done = bf16[1024,512]{1,0:T(8,128)(2,1)} async-done(((bf16[256,512]{1,0:T(8,128)(2,1)}), bf16[1024,512]{1,0:T(8,128)(2,1)}) %all-gather.4.cloned.1.call-update) | async-done | bytes 1048592 | tf_op jit(solution)/shard_map/all_gather | solution.py:89
  41.5 1.5 copy.26
  43.0 0.7 fusion.35
  43.7 0.9 fusion.54
  44.6 1.1 fusion.1
  45.7 0.9 fusion.20
  46.5 0.0 copy-start.1
  46.6 0.0 copy-done
  46.6 1.5 convolution_convert_fusion
  48.0 0.0 copy-start.2
  48.0 0.0 all-reduce.2.cloned.1.call-update
  48.1 0.0 all-gather.6.cloned.1.call-start
  48.1 0.7 all-gather.6.cloned.1.call-update
  48.8 0.0 all-gather.8.cloned.1.call-start
  48.9 0.5 all-gather.8.cloned.1.call-update
  49.4 0.0 reduce-scatter.2.cloned.1.call-start
  49.4 34.2 %all-reduce.2.cloned.1.call-done = bf16[256,2048]{1,0:T(8,128)(2,1)} async-done(((bf16[256,2048]{1,0:T(8,128)(2,1)}), bf16[256,2048]{1,0:T(8,128)(2,1)}) %all-reduce.2.cloned.1.call-update) | async-done | bytes 1048592 | tf_op jit(solution)/shard_map/psum | solution.py:114
  83.6 0.0 copy-done.1
  83.6 1.7 fusion.5
  85.4 150.0 %all-gather.6.cloned.1.call-done = bf16[2048,2048]{1,0:T(8,128)(2,1)} async-done(((bf16[512,2048]{1,0:T(8,128)(2,1)}), bf16[2048,2048]{1,0:T(8,128)(2,1)}) %all-gather.6.cloned.1.call-update) | async-done | bytes 8388624 | tf_op jit(solution)/shard_map/all_gather | solution.py:122
  235.3 149.3 %all-gather.8.cloned.1.call-done = bf16[2048,2048]{1,0:T(8,128)(2,1)} async-done(((bf16[2048,512]{1,0:T(8,128)(2,1)}), bf16[2048,2048]{1,0:T(8,128)(2,1)}) %all-gather.8.cloned.1.call-update) | async-done | bytes 8388624 | tf_op jit(solution)/shard_map/all_gather | solution.py:128
  384.6 0.0 copy-done.2
  384.6 11.3 %convolution_convert_fusion.1 = bf16[256,2048]{1,0:T(8,128)(2,1)} fusion(bf16[2048,2048]{1,0:T(8,128)(2,1)} %all-gather.8.cloned.1.call-done, bf16[2048,2048]{1,0:T(8,128)(2,1)} %all-gather.6.cloned.1.call-done, bf16[256,2048]{1,0:T(8,128)(2,1)S(1)} %get-tuple-element.22, f32[2048]{0:T(1024)S(1)} %copy-done.2, f32[256]{0:T(256)S(1)} %add_rsqrt_fusion), kind=kOutput, calls=%fused_computation.11 | convolution fusion | flops 4299161600 | bytes 18883584 | tf_op jit(solution)/shard_map/dot_general | solution.py:126
  395.9 0.0 reduce-scatter.2.cloned.1.call-update
  395.9 23.1 %reduce-scatter.2.cloned.1.call-done = bf16[64,2048]{1,0:T(8,128)(2,1)} async-done(((bf16[256,2048]{1,0:T(8,128)(2,1)}), bf16[64,2048]{1,0:T(8,128)(2,1)}) %reduce-scatter.2.cloned.1.call-update) | async-done | bytes 262160 | tf_op jit(solution)/shard_map/reduce_scatter | solution.py:131
  419.0 1.7 add_convert_fusion.1
  (8 shorter events, 0.1 us)
Async XLA Ops:
  6.5 40.0 %copy-start = (bf16[256,2048]{1,0:T(8,128)(2,1)S(1)}, bf16[256,2048]{1,0:T(8,128)(2,1)}, u32[]{:S(2)}) copy-start(bf16[256,2048]{1,0:T(8,128)(2,1)} %param.20) | copy-start | bytes 3145732
  6.5 34.9 %all-gather.4.cloned.1.call-start = ((), (), s32[]{:S(2)}) async-start(), calls=%async_computation.1 | async-start | bytes 1310720 | tf_op jit(solution)/shard_map/all_gather | solution.py:89
  9.9 73.7 %all-reduce.2.cloned.1.call-start = ((), (), s32[]{:S(2)}) async-start(), calls=%async_computation.2 | async-start | bytes 2097152 | tf_op jit(solution)/shard_map/psum | solution.py:114
  46.5 37.1 %copy-start.1 = (bf16[256,2048]{1,0:T(8,128)(2,1)S(1)}, bf16[256,2048]{1,0:T(8,128)(2,1)}, u32[]{:S(2)}) copy-start(bf16[256,2048]{1,0:T(8,128)(2,1)} %param.12) | copy-start | bytes 3145732
  48.0 336.6 %copy-start.2 = (f32[2048]{0:T(1024)S(1)}, f32[2048]{0:T(1024)}, u32[]{:S(2)}) copy-start(f32[2048]{0:T(1024)} %param.21) | copy-start | bytes 24580
  48.1 187.3 %all-gather.6.cloned.1.call-start = ((), (), s32[]{:S(2)}) async-start(), calls=%async_computation.3 | async-start | bytes 10485760 | tf_op jit(solution)/shard_map/all_gather | solution.py:122
  48.8 335.8 %all-gather.8.cloned.1.call-start = ((), (), s32[]{:S(2)}) async-start(), calls=%async_computation.4 | async-start | bytes 10485760 | tf_op jit(solution)/shard_map/all_gather | solution.py:128
  49.4 369.6 %reduce-scatter.2.cloned.1.call-start = ((), (), s32[]{:S(2)}) async-start(), calls=%async_computation.5 | async-start | bytes 1310720 | tf_op jit(solution)/shard_map/reduce_scatter | solution.py:131
Sparse Core Ops, SparseCore 0:
  10.1 31.3 all-gather.3
  48.2 35.4 all-reduce.1
  85.2 150.0 all-gather.5
  236.8 147.7 all-gather.7
  396.0 22.9 reduce-scatter.1
where the time goes:
time: 428 us; the launch traced here: 427 us
  waiting for transfers between devices  369 us (86%)
  matrix products  19.1 us (4%)
  blocking collectives  15.3 us (4%)
  between operations  13.2 us (3%)
  other arithmetic  8.5 us (2%)
    all_gather x1, waiting for transfers between devices, on_device(): lax.all_gather(feed_up, 'sp', axis=0, tiled=True)  150 us
    all_gather x1, waiting for transfers between devices, on_device(): lax.all_gather(feed_down, 'sp', axis=1, tiled=True)  149 us
    psum x1, waiting for transfers between devices, on_device(): lax.psum(jnp.dot(mixed, out_proj, preferred_element_type=jnp.float32).ast...  34.2 us
    reduce_scatter x1, waiting for transfers between devices, on_device(): lax.psum_scatter(partial_sum.astype(jnp.bfloat16), 'tp', scatter_dimensio...  23.1 us
    all_gather x1, blocking collectives, on_device(): lax.all_gather(key_rope, 'sp', axis=0, tiled=True)  15.3 us
    dot_general x1, matrix products, on_device(): jnp.dot(activated, lax.all_gather(feed_down, 'sp', axis=1, tiled=True), p...  11.3 us
    all_gather x1, waiting for transfers between devices, on_device(): lax.all_gather(own_keys, 'sp', axis=0, tiled=True)  11.1 us
  transfers between devices with their start and end apart: 5, of which 5 were waited for; matrix products, arithmetic and copies ran while one was open for 2% of the time, Pallas kernels for 0%

commit v1 on v0

--- a/solution.py
+++ b/solution.py
@@ -7,6 +7,11 @@
 QUERY_KEY_PLAIN = 64
 QUERY_KEY_ROTARY = 32
 VALUE_HEAD_SIZE = 64
+
+
+def summed_here(x, mesh_axis):
+    parts = lax.all_gather(x, mesh_axis)
+    return jnp.sum(parts, axis=0)
 
 
 def normalize(values, gain):
@@ -111,7 +116,7 @@
     )
     share = tokens_here // lax.axis_size("tp")
     lead = lax.axis_index("tp") * share
-    branch = lax.psum(
+    branch = summed_here(
         jnp.dot(mixed, out_proj, preferred_element_type=jnp.float32).astype(jnp.bfloat16), "tp"
     ).astype(jnp.float32)
     middle = (hidden_in.astype(jnp.float32) + branch).astype(jnp.bfloat16)

time: 428 us -> 425 us (level)
  waiting for transfers between devices: 369 us -> 363 us
    psum x1 -> x0, waiting for transfers between devices: 34.2 us -> none  [on_device(): lax.psum(jnp.dot(mixed, out_proj, preferred_element_type=jnp.float32).ast...]
    all_gather x0 -> x1, waiting for transfers between devices: none -> 32.4 us  [summed_here(): parts = lax.all_gather(x, mesh_axis)]
where the time goes in v1:
time: 425 us
  waiting for transfers between devices  363 us (85%)
  matrix products  19 us (4%)
  blocking collectives  15.4 us (4%)
  between operations  13.2 us (3%)
  other arithmetic  11.6 us (3%)
    all_gather x1, waiting for transfers between devices, on_device(): lax.all_gather(feed_up, 'sp', axis=0, tiled=True)  149 us
    all_gather x1, waiting for transfers between devices, on_device(): lax.all_gather(feed_down, 'sp', axis=1, tiled=True)  146 us
    all_gather x1, waiting for transfers between devices, summed_here(): parts = lax.all_gather(x, mesh_axis)  32.4 us
    reduce_scatter x1, waiting for transfers between devices, on_device(): lax.psum_scatter(partial_sum.astype(jnp.bfloat16), 'tp', scatter_dimensio...  23.1 us
    all_gather x1, blocking collectives, on_device(): lax.all_gather(key_rope, 'sp', axis=0, tiled=True)  15.4 us
    dot_general x1, matrix products, on_device(): jnp.dot(activated, lax.all_gather(feed_down, 'sp', axis=1, tiled=True), p...  11.3 us
    all_gather x1, waiting for transfers between devices, on_device(): lax.all_gather(own_keys, 'sp', axis=0, tiled=True)  11 us
  transfers between devices with their start and end apart: 5, of which 5 were waited for; matrix products, arithmetic and copies ran while one was open for 2% of the time, Pallas kernels for 0%

profile of v1, /device:TPU:0, one launch (start us, length us, event | category | flops | bytes accessed | tf_op | source)
XLA Modules:
  0.0 424.9 jit_solution(8367574819751764297)
XLA Ops:
  6.5 0.0 copy-start
  6.5 0.0 all-gather.6.cloned.1.call-start
  6.5 1.2 fusion.31
  7.7 2.2 convolution_convert_fusion.2
  9.9 0.0 all-gather.6.cloned.1.call-update
  9.9 0.0 all-gather.12.cloned.1.call-start
  10.0 0.7 convert_element_type.77
  10.7 0.7 slice.45
  11.4 0.1 multiply_cosine_fusion
  11.6 0.7 pad_maximum_fusion
  12.3 15.4 %all_gather.19 = bf16[1024,32]{0,1:T(8,128)(2,1)S(1)} all-gather(bf16[256,32]{0,1:T(8,128)(2,1)S(1)} %get-tuple-element.26), channel_id=1, replica_groups=mesh['grp'=2,'sp'=4,'tp'=4] {'sp'}, dimensions={0}, use_global_device_ids=true | all-gather | bytes 81920 | tf_op jit(solution)/shard_map/all_gather | solution.py:95
  27.7 1.2 fusion.26
  28.8 1.6 fusion.37
  30.5 11.0 %all-gather.6.cloned.1.call-done = bf16[1024,512]{1,0:T(8,128)(2,1)} async-done(((bf16[256,512]{1,0:T(8,128)(2,1)}), bf16[1024,512]{1,0:T(8,128)(2,1)}) %all-gather.6.cloned.1.call-update) | async-done | bytes 1048592 | tf_op jit(solution)/shard_map/all_gather | solution.py:94
  41.5 1.5 copy.26
  43.0 0.7 fusion.35
  43.7 0.9 fusion.54
  44.6 1.1 fusion.1
  45.7 0.9 fusion.20
  46.5 0.0 copy-done
  46.5 1.4 convolution_convert_fusion
  48.0 0.0 all-gather.12.cloned.1.call-update
  48.0 0.0 all-gather.10.cloned.1.call-start
  48.1 0.7 all-gather.10.cloned.1.call-update
  48.8 0.0 all-gather.8.cloned.1.call-start
  48.8 0.5 all-gather.8.cloned.1.call-update
  49.3 0.0 reduce-scatter.2.cloned.1.call-start
  49.4 32.4 %all-gather.12.cloned.1.call-done = bf16[1024,2048]{1,0:T(8,128)(2,1)} async-done(((bf16[256,2048]{1,0:T(8,128)(2,1)}), bf16[1024,2048]{1,0:T(8,128)(2,1)}) %all-gather.12.cloned.1.call-update) | async-done | bytes 4194320 | tf_op jit(solution)/shard_map/all_gather | solution.py:13
  81.7 0.0 copy-start.1
  81.8 3.1 reduce_sum.55
  84.8 1.7 fusion.5
  86.6 146.4 %all-gather.10.cloned.1.call-done = bf16[2048,2048]{1,0:T(8,128)(2,1)} async-done(((bf16[2048,512]{1,0:T(8,128)(2,1)}), bf16[2048,2048]{1,0:T(8,128)(2,1)}) %all-gather.10.cloned.1.call-update) | async-done | bytes 8388624 | tf_op jit(solution)/shard_map/all_gather | solution.py:133
  233.0 149.3 %all-gather.8.cloned.1.call-done = bf16[2048,2048]{1,0:T(8,128)(2,1)} async-done(((bf16[512,2048]{1,0:T(8,128)(2,1)}), bf16[2048,2048]{1,0:T(8,128)(2,1)}) %all-gather.8.cloned.1.call-update) | async-done | bytes 8388624 | tf_op jit(solution)/shard_map/all_gather | solution.py:127
  382.2 0.0 copy-done.1
  382.2 11.3 %convolution_convert_fusion.1 = bf16[256,2048]{1,0:T(8,128)(2,1)} fusion(bf16[2048,2048]{1,0:T(8,128)(2,1)} %all-gather.10.cloned.1.call-done, bf16[2048,2048]{1,0:T(8,128)(2,1)} %all-gather.8.cloned.1.call-done, bf16[256,2048]{1,0:T(8,128)(2,1)S(1)} %get-tuple-element.22, f32[2048]{0:T(1024)S(1)} %copy-done.1, f32[256]{0:T(256)S(1)} %add_rsqrt_fusion), kind=kOutput, calls=%fused_computation.11 | convolution fusion | flops 4299161600 | bytes 18883584 | tf_op jit(solution)/shard_map/dot_general | solution.py:131
  393.5 0.0 reduce-scatter.2.cloned.1.call-update
  393.5 23.1 %reduce-scatter.2.cloned.1.call-done = bf16[64,2048]{1,0:T(8,128)(2,1)} async-done(((bf16[256,2048]{1,0:T(8,128)(2,1)}), bf16[64,2048]{1,0:T(8,128)(2,1)}) %reduce-scatter.2.cloned.1.call-update) | async-done | bytes 262160 | tf_op jit(solution)/shard_map/reduce_scatter | solution.py:136
  416.7 1.7 add_convert_fusion.1
  (8 shorter events, 0.1 us)
Async XLA Ops:
  6.5 40.0 %copy-start = (bf16[256,2048]{1,0:T(8,128)(2,1)S(1)}, bf16[256,2048]{1,0:T(8,128)(2,1)}, u32[]{:S(2)}) copy-start(bf16[256,2048]{1,0:T(8,128)(2,1)} %param.20) | copy-start | bytes 3145732
  6.5 34.9 %all-gather.6.cloned.1.call-start = ((), (), s32[]{:S(2)}) async-start(), calls=%async_computation.1 | async-start | bytes 1310720 | tf_op jit(solution)/shard_map/all_gather | solution.py:94
  9.9 71.8 %all-gather.12.cloned.1.call-start = ((), (), s32[]{:S(2)}) async-start(), calls=%async_computation.5 | async-start | bytes 5242880 | tf_op jit(solution)/shard_map/all_gather | solution.py:13
  48.0 185.0 %all-gather.10.cloned.1.call-start = ((), (), s32[]{:S(2)}) async-start(), calls=%async_computation.3 | async-start | bytes 10485760 | tf_op jit(solution)/shard_map/all_gather | solution.py:133
  48.8 333.5 %all-gather.8.cloned.1.call-start = ((), (), s32[]{:S(2)}) async-start(), calls=%async_computation.2 | async-start | bytes 10485760 | tf_op jit(solution)/shard_map/all_gather | solution.py:127
  49.3 367.3 %reduce-scatter.2.cloned.1.call-start = ((), (), s32[]{:S(2)}) async-start(), calls=%async_computation.4 | async-start | bytes 1310720 | tf_op jit(solution)/shard_map/reduce_scatter | solution.py:136
  81.7 300.5 %copy-start.1 = (f32[2048]{0:T(1024)S(1)}, f32[2048]{0:T(1024)}, u32[]{:S(2)}) copy-start(f32[2048]{0:T(1024)} %param.21) | copy-start | bytes 24580
Sparse Core Ops, SparseCore 0:
  10.1 31.3 all-gather.5
  48.1 33.5 all-gather.11
  83.3 149.6 all-gather.9
  234.4 147.7 all-gather.7
  393.7 22.9 reduce-scatter.1
